TPU v7x, 32 devices: a whole 2x2x4 slice. The times are simulated.
32 devices in a mesh: sp: 16 (over z, y, x), tp: 2 (over core).
Axes of the slice: x: 2, y: 2, z: 4, core: 2. Of those that a mesh axis runs over, the one named last changes fastest.
Arguments:
- residual: bfloat16 [3072, 1024], P('sp', 'tp'), may hold values from -6 to 6
- query_first: bfloat16 [3072, 1024], P('sp', 'tp'), may hold values from -64 to 64
- key_first: bfloat16 [3072, 256], P('sp', 'tp'), may hold values from -20 to 20
- value_first: bfloat16 [3072, 256], P('sp', 'tp'), may hold values from -6 to 6
- documents: int32 [3072], P('sp'), may hold values from 0 to 2, as said below
- bias_first: float32 [16, 513], P('tp'), may hold values from -4 to 4
- out_first: bfloat16 [1024, 1024], P('tp'), may hold values from -0.75 to 0.75
- norm_gain: float32 [1024], replicated, may hold values from 0.1 to 1.9
- query_w: bfloat16 [1024, 1024], P(None, 'tp'), may hold values from -0.1875 to 0.1875
- key_w: bfloat16 [1024, 256], P(None, 'tp'), may hold values from -0.1875 to 0.1875
- value_w: bfloat16 [1024, 256], P(None, 'tp'), may hold values from -0.1875 to 0.1875
- bias_second: float32 [16, 513], P('tp'), may hold values from -4 to 4
- out_second: bfloat16 [1024, 1024], P('tp'), may hold values from -0.75 to 0.75
Outputs:
- layer_two: bfloat16 [3072, 1024], P('sp', 'tp')
Inputs may be any that keep to these rules, and one draw needn't show every extreme that they name: Document numbers start at 0, never fall, and rise by one at the first position of each document; there are exactly 3 documents, each of at least 896 positions.
All inputs are finite; a program needn't handle non-finite values.
Results may differ from a plain program's by a relative error of at most 0.017.
Values may be sent and summed in bfloat16 or wider, within the bound.
A program may use at most 64 MiB of HBM per device.

v0:
```python
import jax
import jax.numpy as jnp
from jax import lax
from jax.sharding import PartitionSpec as P

HEAD_SIZE = 64
SEG = 64
PAST = 4
REL_CLIP = 256


eps = 1e-06


def from_behind(block, axis, distance):
    devices = range(lax.axis_size(axis))
    route = [(i - distance, i) for i in devices if i - distance in devices]
    return lax.ppermute(block, axis, route)


def bias_block(bias_table):
    span_rows = PAST * SEG
    band_rows = SEG * (PAST + 1)
    lowest = -(SEG - 1)
    highest = SEG - 1 + span_rows
    table_cols = bias_table.shape[1]
    left_count = max(0, -REL_CLIP - lowest)
    right_count = max(0, highest - REL_CLIP)
    first_col = max(0, lowest + REL_CLIP)
    last_col = min(table_cols, highest + REL_CLIP + 1)
    heads_local = bias_table.shape[0]
    pieces = []
    pieces.append(bias_table[:, first_col:last_col])
    pieces.append(jnp.broadcast_to(bias_table[:, table_cols - 1 :], (heads_local, right_count)))
    extended = jnp.concatenate(pieces, axis=1)[:, ::-1]
    length = extended.shape[1]
    rows = [
        extended[:, length - band_rows - query_row : length - query_row] for query_row in range(SEG)
    ]
    return jnp.stack(rows, axis=1)


def collect_prior(tok_rows, sender):
    span_rows = PAST * SEG
    hop_count = (span_rows + tok_rows - 1) // tok_rows
    arrived = []
    for distance in range(hop_count, 0, -1):
        needed = min(tok_rows, span_rows - (distance - 1) * tok_rows)
        arrived.append(sender(tok_rows - needed, distance))
    return arrived


def join_member(arrived, member):
    return jnp.concatenate([received[member] for received in arrived], axis=0)


def normalize(rows, norm_gain):
    rows_wide = rows.astype(jnp.float32)
    scale = lax.rsqrt(jnp.mean(rows_wide * rows_wide, axis=1, keepdims=True) + eps)
    return (rows_wide * scale * norm_gain).astype(jnp.bfloat16)


def make_bands(extended, segments):
    blocks = extended.reshape((segments + PAST, SEG) + extended.shape[1:])
    return jnp.concatenate([blocks[lag : lag + segments] for lag in range(PAST + 1)], axis=1)


def attend(queries, keys_ext, values_ext, parity_ext, valid_ext, parity_own, bias_table):
    tok_rows = queries.shape[0]
    segments = tok_rows // SEG
    band_rows = SEG * (PAST + 1)
    kv_local = keys_ext.shape[1] // HEAD_SIZE
    group_size = queries.shape[1] // HEAD_SIZE // kv_local
    key_bands = make_bands(keys_ext, segments).reshape(segments, band_rows, kv_local, HEAD_SIZE)
    value_bands = make_bands(values_ext, segments).reshape(segments, band_rows, kv_local, HEAD_SIZE)
    parity_bands = make_bands(parity_ext, segments)
    valid_bands = make_bands(valid_ext, segments)
    query_blocks = queries.reshape(segments, SEG, kv_local, group_size, HEAD_SIZE)
    logit_scores = jnp.einsum(
        "sqkgd,sbkd->skgqb", query_blocks, key_bands, preferred_element_type=jnp.float32
    )
    logit_scores = logit_scores * HEAD_SIZE ** (-0.5) + bias_block(bias_table).reshape(
        kv_local, group_size, SEG, band_rows
    )
    allowed = valid_bands[:, None, :] & (
        parity_bands[:, None, :] == parity_own.reshape(segments, SEG)[:, :, None]
    )
    logit_scores = jnp.where(allowed[:, None, None], logit_scores, -jnp.inf)
    largest = jnp.max(logit_scores, axis=-1, keepdims=True)
    softmax_weight = jnp.exp(logit_scores - largest)
    softmax_weight = (softmax_weight / jnp.sum(softmax_weight, axis=-1, keepdims=True)).astype(
        jnp.bfloat16
    )
    blended_output = jnp.einsum(
        "skgqb,sbkd->sqkgd", softmax_weight, value_bands, preferred_element_type=jnp.float32
    )
    return blended_output.astype(jnp.bfloat16).reshape(tok_rows, kv_local * group_size * HEAD_SIZE)


def body(
    residual,
    query_first,
    key_first,
    value_first,
    documents,
    bias_first,
    out_first,
    norm_gain,
    query_w,
    key_w,
    value_w,
    bias_second,
    out_second,
):
    tok_rows = residual.shape[0]
    span_rows = PAST * SEG
    offset = lax.axis_index("sp") * tok_rows
    positions = offset - span_rows + jnp.arange(span_rows + tok_rows, dtype=jnp.int32)
    valid_ext = positions >= 0
    parity_own = (documents % 2).astype(jnp.bfloat16)

    def send_first(first_row, distance):
        return from_behind(
            (key_first[first_row:], value_first[first_row:], parity_own[first_row:]), "sp", distance
        )

    arrived = collect_prior(tok_rows, send_first)
    prior_key = join_member(arrived, 0)
    prior_value = join_member(arrived, 1)
    parity_ext = jnp.concatenate([join_member(arrived, 2), parity_own], axis=0)
    mixed_one = attend(
        query_first,
        jnp.concatenate([prior_key, key_first], axis=0),
        jnp.concatenate([prior_value, value_first], axis=0),
        parity_ext,
        valid_ext,
        parity_own,
        bias_first,
    )
    partial_one = jnp.dot(mixed_one, out_first, preferred_element_type=jnp.float32)
    branch_sum = lax.psum_scatter(
        partial_one.astype(jnp.bfloat16), "tp", scatter_dimension=1, tiled=True
    ).astype(jnp.float32)
    layer_share = (residual.astype(jnp.float32) + branch_sum).astype(jnp.bfloat16)
    full_rows = lax.all_gather(layer_share, "tp", axis=1, tiled=True)
    normed = normalize(full_rows, norm_gain)
    query_two = jnp.dot(normed, query_w, preferred_element_type=jnp.float32).astype(jnp.bfloat16)
    key_two = jnp.dot(normed, key_w, preferred_element_type=jnp.float32).astype(jnp.bfloat16)
    value_two = jnp.dot(normed, value_w, preferred_element_type=jnp.float32).astype(jnp.bfloat16)

    def send_keys(first_row, distance):
        return from_behind((key_two[first_row:], value_two[first_row:]), "sp", distance)

    arrived_two = collect_prior(tok_rows, send_keys)
    prior_key_two = join_member(arrived_two, 0)
    prior_value_two = join_member(arrived_two, 1)
    mixed_two = attend(
        query_two,
        jnp.concatenate([prior_key_two, key_two], axis=0),
        jnp.concatenate([prior_value_two, value_two], axis=0),
        parity_ext,
        valid_ext,
        parity_own,
        bias_second,
    )
    partial_two = jnp.dot(mixed_two, out_second, preferred_element_type=jnp.float32)
    branch_two = lax.psum_scatter(
        partial_two.astype(jnp.bfloat16), "tp", scatter_dimension=1, tiled=True
    ).astype(jnp.float32)
    return (layer_share.astype(jnp.float32) + branch_two).astype(jnp.bfloat16)


def solution(mesh):
    placed = (
        P("sp", "tp"),
        P("sp", "tp"),
        P("sp", "tp"),
        P("sp", "tp"),
        P("sp"),
        P("tp", None),
        P("tp", None),
        P(),
        P(None, "tp"),
        P(None, "tp"),
        P(None, "tp"),
        P("tp", None),
        P("tp", None),
    )
    return jax.shard_map(body, mesh=mesh, in_specs=placed, out_specs=P("sp", "tp"), check_vma=False)
```

profile of v0, /device:TPU:25, one launch (start us, length us, event | category | flops | bytes accessed | tf_op | source)
XLA Modules:
  0.0 158.4 jit_solution(7395406331355812803)
XLA Ops:
  6.5 1.3 fusion.172
  7.8 3.1 %collective-permute-start.3 = (bf16[192]{0:T(256)(128)(2,1)}, bf16[192]{0:T(256)(128)(2,1)S(1)}, u32[]{:S(2)}, u32[]{:S(2)}) collective-permute-start(bf16[192]{0:T(256)(128)(2,1)} %fusion.172), channel_id=1, source_target_pairs={{0,2},{2,4},{4,6},{6,8},{8,10},{10,12},{12,14},{14,16},{16,18},{18... | collective-permute-start | bytes 1160 | tf_op jit(solution)/shard_map/ppermute | solution.py:18
  10.9 1.2 slice.952
  12.1 3.1 %collective-permute-start.2 = (bf16[64]{0:T(256)(128)(2,1)}, bf16[64]{0:T(256)(128)(2,1)}, u32[]{:S(2)}, u32[]{:S(2)}) collective-permute-start(bf16[64]{0:T(256)(128)(2,1)} %slice.952), channel_id=1, source_target_pairs={{0,4},{2,6},{4,8},{6,10},{8,12},{10,14},{12,16},{14,18},{16,20},{1... | collective-permute-start | bytes 392 | tf_op jit(solution)/shard_map/ppermute | solution.py:18
  15.3 1.9 %collective-permute-start.5 = (bf16[192,128]{1,0:T(8,128)(2,1)}, bf16[192,128]{1,0:T(8,128)(2,1)S(1)}, u32[]{:S(2)}, u32[]{:S(2)}) collective-permute-start(bf16[192,128]{1,0:T(8,128)(2,1)} %param.15), channel_id=1, source_target_pairs={{0,2},{2,4},{4,6},{6,8},{8,10},{10,12},{12,14},{14,16},{16,18},{18... | collective-permute-start | bytes 147464 | tf_op jit(solution)/shard_map/ppermute | solution.py:18
  17.2 1.3 slice.958
  18.5 1.9 %collective-permute-start.4 = (bf16[64,128]{1,0:T(8,128)(2,1)}, bf16[64,128]{1,0:T(8,128)(2,1)}, u32[]{:S(2)}, u32[]{:S(2)}) collective-permute-start(bf16[64,128]{1,0:T(8,128)(2,1)} %slice.958), channel_id=1, source_target_pairs={{0,4},{2,6},{4,8},{6,10},{8,12},{10,14},{12,16},{14,18},{16,20},{1... | collective-permute-start | bytes 49160 | tf_op jit(solution)/shard_map/ppermute | solution.py:18
  20.4 2.5 %collective-permute-start.1 = (bf16[192,128]{1,0:T(8,128)(2,1)}, bf16[192,128]{1,0:T(8,128)(2,1)S(1)}, u32[]{:S(2)}, u32[]{:S(2)}) collective-permute-start(bf16[192,128]{1,0:T(8,128)(2,1)} %param.16), channel_id=1, source_target_pairs={{0,2},{2,4},{4,6},{6,8},{8,10},{10,12},{12,14},{14,16},{16,18},{18... | collective-permute-start | bytes 147464 | tf_op jit(solution)/shard_map/ppermute | solution.py:18
  27.9 0.9 concatenate.135
  28.8 1.3 slice.943
  30.1 0.9 concatenate.122
  70.9 1.3 stack.454
  72.2 1.9 %collective-permute-start = (bf16[64,128]{1,0:T(8,128)(2,1)}, bf16[64,128]{1,0:T(8,128)(2,1)S(1)}, u32[]{:S(2)}, u32[]{:S(2)}) collective-permute-start(bf16[64,128]{1,0:T(8,128)(2,1)} %slice.943), channel_id=1, source_target_pairs={{0,4},{2,6},{4,8},{6,10},{8,12},{10,14},{12,16},{14,18},{16,20},{1... | collective-permute-start | bytes 49160 | tf_op jit(solution)/shard_map/ppermute | solution.py:18
  79.6 3.3 %fusion.192 = (f32[3,2,4,64]{3,2,1,0:T(4,128)S(1)}, f32[3,2,4,64,320]{4,3,2,1,0:T(8,128)}) fusion(f32[2,4,64,320]{3,2,1,0:T(8,128)S(1)} %bitcast.198, pred[3,64,320]{2,1,0:T(8,128)(4,1)} %compare_and_fusion, bf16[3,64,2,4,64]{4,3,2,1,0:T(4,128)(2,1)S(1)} %reshape.400, bf16[3,320,2,64]{1,3,2,0:T(8,128)(2,1)S(1)} %concatenate.136), kind=kOutput, calls=%fused_computation.330 | convolution fusion | flops 65372480 | bytes 3131392 | tf_op jit(solution)/shard_map/sub | solution.py:90
  83.2 2.6 %fusion.8 = bf16[3,64,2,4,64]{1,4,3,2,0:T(8,128)(2,1)S(1)} fusion(f32[3,2,4,64,320]{4,3,2,1,0:T(8,128)} %get-tuple-element.153, f32[3,2,4,64]{3,2,1,0:T(4,128)S(1)} %get-tuple-element.152, bf16[3,320,2,64]{1,3,2,0:T(8,128)(2,1)S(1)} %concatenate.123), kind=kOutput, calls=%fused_computation.16 | convolution fusion | flops 63995904 | bytes 2414592 | tf_op jit(solution)/shard_map/skgqb,sbkd->sqkgd/dot_general | solution.py:94
  86.3 1.1 convolution_convert_fusion.2
  104.0 1.3 stack.519
  105.4 1.1 add_convert_fusion.1
  106.5 4.4 %all_gather.3 = bf16[192,1024]{1,0:T(8,128)(2,1)S(1)} all-gather(bf16[192,512]{1,0:T(8,128)(2,1)S(1)} %add_convert_fusion.1), channel_id=1, replica_groups=mesh['sp'=16,'tp'=2] {'tp'}, dimensions={1}, use_global_device_ids=true | all-gather | bytes 589824 | tf_op jit(solution)/shard_map/all_gather | solution.py:145
  111.4 1.9 %collective-permute-start.7 = (bf16[192,128]{1,0:T(8,128)(2,1)S(1)}, bf16[192,128]{1,0:T(8,128)(2,1)S(1)}, u32[]{:S(2)}, u32[]{:S(2)}) collective-permute-start(bf16[192,128]{1,0:T(8,128)(2,1)S(1)} %convolution_convert_fusion.6), channel_id=1, source_target_pairs={{0,2},{2,4},{4,6},{6,8},{8,10},{10,12},{12,14},{14,16},{16,18},{18... | collective-permute-start | bytes 147464 | tf_op jit(solution)/shard_map/ppermute | solution.py:18
  113.3 1.9 %collective-permute-start.6 = (bf16[64,128]{1,0:T(8,128)(2,1)S(1)}, bf16[64,128]{1,0:T(8,128)(2,1)S(1)}, u32[]{:S(2)}, u32[]{:S(2)}) collective-permute-start(bf16[64,128]{1,0:T(8,128)(2,1)S(1)} %slice.1356), channel_id=1, source_target_pairs={{0,4},{2,6},{4,8},{6,10},{8,12},{10,14},{12,16},{14,18},{16,20},{1... | collective-permute-start | bytes 49160 | tf_op jit(solution)/shard_map/ppermute | solution.py:18
  115.2 1.3 convolution_convert_fusion.5
  116.5 1.9 %collective-permute-start.9 = (bf16[192,128]{1,0:T(8,128)(2,1)S(1)}, bf16[192,128]{1,0:T(8,128)(2,1)S(1)}, u32[]{:S(2)}, u32[]{:S(2)}) collective-permute-start(bf16[192,128]{1,0:T(8,128)(2,1)S(1)} %convolution_convert_fusion.5), channel_id=1, source_target_pairs={{0,2},{2,4},{4,6},{6,8},{8,10},{10,12},{12,14},{14,16},{16,18},{18... | collective-permute-start | bytes 147464 | tf_op jit(solution)/shard_map/ppermute | solution.py:18
  119.2 1.9 %collective-permute-start.8 = (bf16[64,128]{1,0:T(8,128)(2,1)S(1)}, bf16[64,128]{1,0:T(8,128)(2,1)S(1)}, u32[]{:S(2)}, u32[]{:S(2)}) collective-permute-start(bf16[64,128]{1,0:T(8,128)(2,1)S(1)} %slice.1359), channel_id=1, source_target_pairs={{0,4},{2,6},{4,8},{6,10},{8,12},{10,14},{12,16},{14,18},{16,20},{1... | collective-permute-start | bytes 49160 | tf_op jit(solution)/shard_map/ppermute | solution.py:18
  122.5 3.3 %collective-permute-done.8 = bf16[64,128]{1,0:T(8,128)(2,1)S(1)} collective-permute-done((bf16[64,128]{1,0:T(8,128)(2,1)S(1)}, bf16[64,128]{1,0:T(8,128)(2,1)S(1)}, u32[]{:S(2)}, u32[]{:S(2)}) %collective-permute-start.8) | collective-permute-done | bytes 16416 | tf_op jit(solution)/shard_map/ppermute | solution.py:18
  127.1 0.9 concatenate.148
  128.1 0.9 concatenate.153
  129.0 3.3 %fusion.197 = (f32[3,2,4,64]{3,2,1,0:T(4,128)S(1)}, f32[3,2,4,64,320]{4,3,2,1,0:T(8,128)}) fusion(f32[2,4,64,320]{3,2,1,0:T(8,128)S(1)} %bitcast.199, pred[3,64,320]{2,1,0:T(8,128)(4,1)} %compare_and_fusion, bf16[3,64,2,4,64]{4,3,2,1,0:T(4,128)(2,1)S(1)} %reshape.402, bf16[3,320,2,64]{1,3,2,0:T(8,128)(2,1)} %concatenate.153), kind=kOutput, calls=%fused_computation.331 | convolution fusion | flops 65372480 | bytes 3131392 | tf_op jit(solution)/shard_map/sub | solution.py:90
  132.6 2.7 %fusion.9 = bf16[3,64,2,4,64]{1,4,3,2,0:T(8,128)(2,1)S(1)} fusion(f32[3,2,4,64,320]{4,3,2,1,0:T(8,128)} %get-tuple-element.155, f32[3,2,4,64]{3,2,1,0:T(4,128)S(1)} %get-tuple-element.154, bf16[3,320,2,64]{1,3,2,0:T(8,128)(2,1)S(1)} %concatenate.145), kind=kOutput, calls=%fused_computation.17 | convolution fusion | flops 63995904 | bytes 2414592 | tf_op jit(solution)/shard_map/skgqb,sbkd->sqkgd/dot_general | solution.py:94
  135.8 1.1 convolution_convert_fusion
  137.0 12.9 %reduce-scatter.5.cloned.1.call-done = bf16[192,512]{1,0:T(8,128)(2,1)} async-done(((bf16[192,1024]{1,0:T(8,128)(2,1)}), bf16[192,512]{1,0:T(8,128)(2,1)}) %reduce-scatter.5.cloned.1.call-update) | async-done | bytes 196624 | tf_op jit(solution)/shard_map/reduce_scatter | solution.py:167
  149.9 1.7 %add_convert_fusion = bf16[192,512]{1,0:T(8,128)(2,1)} fusion(bf16[192,512]{1,0:T(8,128)(2,1)} %reduce-scatter.5.cloned.1.call-done, bf16[192,512]{1,0:T(8,128)(2,1)S(1)} %add_convert_fusion.1), kind=kLoop, calls=%fused_computation.38 | loop fusion | flops 393216 | bytes 589824 | tf_op jit(solution)/shard_map/convert_element_type | solution.py:170
  (556 shorter events, 71.4 us)
Async XLA Ops:
  6.5 79.8 %copy-start = (bf16[512,1024]{1,0:T(8,128)(2,1)S(1)}, bf16[512,1024]{1,0:T(8,128)(2,1)}, u32[]{:S(2)}) copy-start(bf16[512,1024]{1,0:T(8,128)(2,1)} %param.19) | copy-start | bytes 3145732
  6.5 98.8 %reduce-scatter.3.cloned.1.call-start = ((), (), s32[]{:S(2)}) async-start(), calls=%async_computation.2 | async-start | bytes 589824 | tf_op jit(solution)/shard_map/reduce_scatter | solution.py:141
  7.8 64.4 %collective-permute-start.3 = (bf16[192]{0:T(256)(128)(2,1)}, bf16[192]{0:T(256)(128)(2,1)S(1)}, u32[]{:S(2)}, u32[]{:S(2)}) collective-permute-start(bf16[192]{0:T(256)(128)(2,1)} %fusion.172), channel_id=1, source_target_pairs={{0,2},{2,4},{4,6},{6,8},{8,10},{10,12},{12,14},{14,16},{16,18},{18... | collective-permute-start | bytes 1160 | tf_op jit(solution)/shard_map/ppermute | solution.py:18
  12.1 62.1 %collective-permute-start.2 = (bf16[64]{0:T(256)(128)(2,1)}, bf16[64]{0:T(256)(128)(2,1)}, u32[]{:S(2)}, u32[]{:S(2)}) collective-permute-start(bf16[64]{0:T(256)(128)(2,1)} %slice.952), channel_id=1, source_target_pairs={{0,4},{2,6},{4,8},{6,10},{8,12},{10,14},{12,16},{14,18},{16,20},{1... | collective-permute-start | bytes 392 | tf_op jit(solution)/shard_map/ppermute | solution.py:18
  15.3 60.7 %collective-permute-start.5 = (bf16[192,128]{1,0:T(8,128)(2,1)}, bf16[192,128]{1,0:T(8,128)(2,1)S(1)}, u32[]{:S(2)}, u32[]{:S(2)}) collective-permute-start(bf16[192,128]{1,0:T(8,128)(2,1)} %param.15), channel_id=1, source_target_pairs={{0,2},{2,4},{4,6},{6,8},{8,10},{10,12},{12,14},{14,16},{16,18},{18... | collective-permute-start | bytes 147464 | tf_op jit(solution)/shard_map/ppermute | solution.py:18
  18.5 57.4 %collective-permute-start.4 = (bf16[64,128]{1,0:T(8,128)(2,1)}, bf16[64,128]{1,0:T(8,128)(2,1)}, u32[]{:S(2)}, u32[]{:S(2)}) collective-permute-start(bf16[64,128]{1,0:T(8,128)(2,1)} %slice.958), channel_id=1, source_target_pairs={{0,4},{2,6},{4,8},{6,10},{8,12},{10,14},{12,16},{14,18},{16,20},{1... | collective-permute-start | bytes 49160 | tf_op jit(solution)/shard_map/ppermute | solution.py:18
  20.4 58.0 %collective-permute-start.1 = (bf16[192,128]{1,0:T(8,128)(2,1)}, bf16[192,128]{1,0:T(8,128)(2,1)S(1)}, u32[]{:S(2)}, u32[]{:S(2)}) collective-permute-start(bf16[192,128]{1,0:T(8,128)(2,1)} %param.16), channel_id=1, source_target_pairs={{0,2},{2,4},{4,6},{6,8},{8,10},{10,12},{12,14},{14,16},{16,18},{18... | collective-permute-start | bytes 147464 | tf_op jit(solution)/shard_map/ppermute | solution.py:18
  35.2 19.4 %copy-start.5 = (bf16[192,512]{1,0:T(8,128)(2,1)S(1)}, bf16[192,512]{1,0:T(8,128)(2,1)}, u32[]{:S(2)}) copy-start(bf16[192,512]{1,0:T(8,128)(2,1)} %param.14) | copy-start | bytes 589828
  52.4 24.2 %copy-start.2 = (bf16[192,128]{1,0:T(8,128)(2,1)S(1)}, bf16[192,128]{1,0:T(8,128)(2,1)}, u32[]{:S(2)}) copy-start(bf16[192,128]{1,0:T(8,128)(2,1)} %param.15) | copy-start | bytes 147460
  59.0 19.5 %copy-start.3 = (bf16[192,128]{1,0:T(8,128)(2,1)S(1)}, bf16[192,128]{1,0:T(8,128)(2,1)}, u32[]{:S(2)}) copy-start(bf16[192,128]{1,0:T(8,128)(2,1)} %param.16) | copy-start | bytes 147460
  72.2 6.2 %collective-permute-start = (bf16[64,128]{1,0:T(8,128)(2,1)}, bf16[64,128]{1,0:T(8,128)(2,1)S(1)}, u32[]{:S(2)}, u32[]{:S(2)}) collective-permute-start(bf16[64,128]{1,0:T(8,128)(2,1)} %slice.943), channel_id=1, source_target_pairs={{0,4},{2,6},{4,8},{6,10},{8,12},{10,14},{12,16},{14,18},{16,20},{1... | collective-permute-start | bytes 49160 | tf_op jit(solution)/shard_map/ppermute | solution.py:18
  87.5 16.4 %copy-start.8 = (f32[1,2,4,1,320]{4,3,2,1,0:T(1,128)S(1)}, f32[1,2,4,1,320]{4,3,2,1,0:T(1,128)}, u32[]{:S(2)}) copy-start(f32[1,2,4,1,320]{4,3,2,1,0:T(1,128)} %stack.637) | copy-start | bytes 30724
  87.5 16.4 %copy-start.9 = (f32[1,2,4,1,320]{4,3,2,1,0:T(1,128)S(1)}, f32[1,2,4,1,320]{4,3,2,1,0:T(1,128)}, u32[]{:S(2)}) copy-start(f32[1,2,4,1,320]{4,3,2,1,0:T(1,128)} %stack.585) | copy-start | bytes 30724
  87.5 16.4 %copy-start.10 = (f32[1,2,4,1,320]{4,3,2,1,0:T(1,128)S(1)}, f32[1,2,4,1,320]{4,3,2,1,0:T(1,128)}, u32[]{:S(2)}) copy-start(f32[1,2,4,1,320]{4,3,2,1,0:T(1,128)} %stack.586) | copy-start | bytes 30724
  87.5 16.4 %copy-start.11 = (f32[1,2,4,1,320]{4,3,2,1,0:T(1,128)S(1)}, f32[1,2,4,1,320]{4,3,2,1,0:T(1,128)}, u32[]{:S(2)}) copy-start(f32[1,2,4,1,320]{4,3,2,1,0:T(1,128)} %stack.587) | copy-start | bytes 30724
  87.5 16.4 %copy-start.12 = (f32[1,2,4,1,320]{4,3,2,1,0:T(1,128)S(1)}, f32[1,2,4,1,320]{4,3,2,1,0:T(1,128)}, u32[]{:S(2)}) copy-start(f32[1,2,4,1,320]{4,3,2,1,0:T(1,128)} %stack.588) | copy-start | bytes 30724
  87.5 16.4 %copy-start.13 = (f32[1,2,4,1,320]{4,3,2,1,0:T(1,128)S(1)}, f32[1,2,4,1,320]{4,3,2,1,0:T(1,128)}, u32[]{:S(2)}) copy-start(f32[1,2,4,1,320]{4,3,2,1,0:T(1,128)} %stack.589) | copy-start | bytes 30724
  87.5 16.4 %copy-start.14 = (f32[1,2,4,1,320]{4,3,2,1,0:T(1,128)S(1)}, f32[1,2,4,1,320]{4,3,2,1,0:T(1,128)}, u32[]{:S(2)}) copy-start(f32[1,2,4,1,320]{4,3,2,1,0:T(1,128)} %stack.590) | copy-start | bytes 30724
  87.5 16.4 %copy-start.15 = (f32[1,2,4,1,320]{4,3,2,1,0:T(1,128)S(1)}, f32[1,2,4,1,320]{4,3,2,1,0:T(1,128)}, u32[]{:S(2)}) copy-start(f32[1,2,4,1,320]{4,3,2,1,0:T(1,128)} %stack.591) | copy-start | bytes 30724
  87.5 16.4 %copy-start.16 = (f32[1,2,4,1,320]{4,3,2,1,0:T(1,128)S(1)}, f32[1,2,4,1,320]{4,3,2,1,0:T(1,128)}, u32[]{:S(2)}) copy-start(f32[1,2,4,1,320]{4,3,2,1,0:T(1,128)} %stack.592) | copy-start | bytes 30724
  87.5 16.4 %copy-start.17 = (f32[1,2,4,1,320]{4,3,2,1,0:T(1,128)S(1)}, f32[1,2,4,1,320]{4,3,2,1,0:T(1,128)}, u32[]{:S(2)}) copy-start(f32[1,2,4,1,320]{4,3,2,1,0:T(1,128)} %stack.593) | copy-start | bytes 30724
  87.6 16.4 %copy-start.18 = (f32[1,2,4,1,320]{4,3,2,1,0:T(1,128)S(1)}, f32[1,2,4,1,320]{4,3,2,1,0:T(1,128)}, u32[]{:S(2)}) copy-start(f32[1,2,4,1,320]{4,3,2,1,0:T(1,128)} %stack.594) | copy-start | bytes 30724
  87.6 16.4 %copy-start.19 = (f32[1,2,4,1,320]{4,3,2,1,0:T(1,128)S(1)}, f32[1,2,4,1,320]{4,3,2,1,0:T(1,128)}, u32[]{:S(2)}) copy-start(f32[1,2,4,1,320]{4,3,2,1,0:T(1,128)} %stack.595) | copy-start | bytes 30724
  87.6 16.4 %copy-start.20 = (f32[1,2,4,1,320]{4,3,2,1,0:T(1,128)S(1)}, f32[1,2,4,1,320]{4,3,2,1,0:T(1,128)}, u32[]{:S(2)}) copy-start(f32[1,2,4,1,320]{4,3,2,1,0:T(1,128)} %stack.596) | copy-start | bytes 30724
  87.6 16.4 %copy-start.21 = (f32[1,2,4,1,320]{4,3,2,1,0:T(1,128)S(1)}, f32[1,2,4,1,320]{4,3,2,1,0:T(1,128)}, u32[]{:S(2)}) copy-start(f32[1,2,4,1,320]{4,3,2,1,0:T(1,128)} %stack.597) | copy-start | bytes 30724
  87.6 16.4 %copy-start.22 = (f32[1,2,4,1,320]{4,3,2,1,0:T(1,128)S(1)}, f32[1,2,4,1,320]{4,3,2,1,0:T(1,128)}, u32[]{:S(2)}) copy-start(f32[1,2,4,1,320]{4,3,2,1,0:T(1,128)} %stack.598) | copy-start | bytes 30724
  87.6 16.4 %copy-start.23 = (f32[1,2,4,1,320]{4,3,2,1,0:T(1,128)S(1)}, f32[1,2,4,1,320]{4,3,2,1,0:T(1,128)}, u32[]{:S(2)}) copy-start(f32[1,2,4,1,320]{4,3,2,1,0:T(1,128)} %stack.599) | copy-start | bytes 30724
  87.6 62.3 %reduce-scatter.5.cloned.1.call-start = ((), (), s32[]{:S(2)}) async-start(), calls=%async_computation.3 | async-start | bytes 589824 | tf_op jit(solution)/shard_map/reduce_scatter | solution.py:167
  111.4 10.2 %collective-permute-start.7 = (bf16[192,128]{1,0:T(8,128)(2,1)S(1)}, bf16[192,128]{1,0:T(8,128)(2,1)S(1)}, u32[]{:S(2)}, u32[]{:S(2)}) collective-permute-start(bf16[192,128]{1,0:T(8,128)(2,1)S(1)} %convolution_convert_fusion.6), channel_id=1, source_target_pairs={{0,2},{2,4},{4,6},{6,8},{8,10},{10,12},{12,14},{14,16},{16,18},{18... | collective-permute-start | bytes 147464 | tf_op jit(solution)/shard_map/ppermute | solution.py:18
  113.3 8.2 %collective-permute-start.6 = (bf16[64,128]{1,0:T(8,128)(2,1)S(1)}, bf16[64,128]{1,0:T(8,128)(2,1)S(1)}, u32[]{:S(2)}, u32[]{:S(2)}) collective-permute-start(bf16[64,128]{1,0:T(8,128)(2,1)S(1)} %slice.1356), channel_id=1, source_target_pairs={{0,4},{2,6},{4,8},{6,10},{8,12},{10,14},{12,16},{14,18},{16,20},{1... | collective-permute-start | bytes 49160 | tf_op jit(solution)/shard_map/ppermute | solution.py:18
  116.5 9.3 %collective-permute-start.9 = (bf16[192,128]{1,0:T(8,128)(2,1)S(1)}, bf16[192,128]{1,0:T(8,128)(2,1)S(1)}, u32[]{:S(2)}, u32[]{:S(2)}) collective-permute-start(bf16[192,128]{1,0:T(8,128)(2,1)S(1)} %convolution_convert_fusion.5), channel_id=1, source_target_pairs={{0,2},{2,4},{4,6},{6,8},{8,10},{10,12},{12,14},{14,16},{16,18},{18... | collective-permute-start | bytes 147464 | tf_op jit(solution)/shard_map/ppermute | solution.py:18
  119.2 6.6 %collective-permute-start.8 = (bf16[64,128]{1,0:T(8,128)(2,1)S(1)}, bf16[64,128]{1,0:T(8,128)(2,1)S(1)}, u32[]{:S(2)}, u32[]{:S(2)}) collective-permute-start(bf16[64,128]{1,0:T(8,128)(2,1)S(1)} %slice.1359), channel_id=1, source_target_pairs={{0,4},{2,6},{4,8},{6,10},{8,12},{10,14},{12,16},{14,18},{16,20},{1... | collective-permute-start | bytes 49160 | tf_op jit(solution)/shard_map/ppermute | solution.py:18
  (10 other events, 120.6 us)
Sparse Core Ops, SparseCore 0:
  87.8 11.9 reduce-scatter.2
  137.1 12.7 reduce-scatter.4
where the time goes:
time: 160 us; the launch traced here: 158 us
  local copies, waits for them, and re-layouts  73.5 us (46%)
  starting transfers between devices  22.4 us (14%)
  waiting for transfers between devices  17.1 us (11%)
  matrix products  16.2 us (10%)
  between operations  14.7 us (9%)
  other arithmetic  10.2 us (6%)
  blocking collectives  4.37 us (3%)
    unnamed x316, local copies, waits for them, and re-layouts  40.1 us
    ppermute x10, starting transfers between devices, from_behind(): return lax.ppermute(block, axis, route)  22.1 us
    another operation x130, local copies, waits for them, and re-layouts, bias_block(): return jnp.stack(rows, axis=1)  15.2 us
    reduce_scatter x1, waiting for transfers between devices, body(): lax.psum_scatter(partial_two.astype(jnp.bfloat16), 'tp', scatter_dimensio...  12.9 us
    concatenate x46, local copies, waits for them, and re-layouts, make_bands(): jnp.concatenate([blocks[lag:lag + segments] for lag in range(PAST + 1)],...  8.58 us
    sub x2, matrix products, attend(): softmax_weight = jnp.exp(logit_scores - largest)  6.66 us
    dot_general x2, matrix products, attend(): jnp.einsum('skgqb,sbkd->sqkgd', softmax_weight, value_bands, preferred_el...  5.32 us
    all_gather x1, blocking collectives, body(): full_rows = lax.all_gather(layer_share, 'tp', axis=1, tiled=True)  4.37 us
  transfers between devices with their start and end apart: 12, of which 3 were waited for; matrix products, arithmetic and copies ran while one was open for 48% of the time, Pallas kernels for 0%

commit v1 on v0

v1 whole, which is shorter than its diff:
```python
import functools

import jax
import jax.numpy as jnp
from jax import lax
from jax.experimental import pallas as pl
from jax.experimental.pallas import tpu as pltpu
from jax.sharding import PartitionSpec as P

HEAD_SIZE = 64
SEG = 64
PAST = 4
REL_CLIP = 256
SPAN = PAST * SEG
BAND = SPAN + SEG
LANES = 128
LOG2E = 1.4426950408889634
HIDDEN = -1e30
MESH = pl.DeviceIdType.MESH


eps = 1e-06


def hops_of(tok_rows):
    hops = []
    for distance in range(1, (SPAN + tok_rows - 1) // tok_rows + 1):
        needed = min(tok_rows, SPAN - (distance - 1) * tok_rows)
        hops.append((distance, tok_rows - needed, needed, SPAN - (distance - 1) * tok_rows - needed))
    return hops


def build_bias(table_ref, bias_ref):
    heads_local = table_ref.shape[0]
    group_size = bias_ref.shape[2] // SEG
    lane = lax.broadcasted_iota(jnp.int32, (SEG, LANES), 1)
    low = lane < SEG
    last = REL_CLIP + SPAN

    def tile(head, index):
        if index == 0:
            return jnp.broadcast_to(table_ref[head : head + 1, last : last + 1], (SEG, LANES))
        first = last - index * LANES
        return jnp.broadcast_to(table_ref[head : head + 1, first : first + LANES], (SEG, LANES))

    def piece(head, block, base):
        back = block // 2
        if block % 2 == 0:
            source = jnp.where(low, tile(head, back), tile(head, back + 1))
            shift = base
        else:
            source = tile(head, back + 1)
            shift = (base + SEG) % LANES
        return pltpu.roll(source, shift, 1, stride=1, stride_axis=0)

    for head in range(0, heads_local, 2):
        for block in range(PAST + 1):
            pair = jnp.where(low, piece(head, block, 0), piece(head + 1, block, SEG)) * LOG2E
            group, inner = head // group_size, head % group_size
            bias_ref[group, block * SEG : (block + 1) * SEG, inner * SEG : (inner + 2) * SEG] = pair


def attend(query_ref, kv_ref, bias_ref, mask_ref, mixed_ref):
    tok_rows = query_ref.shape[0]
    kv_local = bias_ref.shape[0]
    group_size = bias_ref.shape[2] // SEG
    kv_width = kv_local * HEAD_SIZE
    for segment in range(tok_rows // SEG):
        rows = slice(segment * SEG, (segment + 1) * SEG)
        band = slice(segment * SEG, segment * SEG + BAND)
        mask = mask_ref[segment]
        mask = jnp.concatenate([mask] * (group_size * SEG // LANES), axis=1)
        for group in range(kv_local):
            keys = kv_ref[band, group * HEAD_SIZE : (group + 1) * HEAD_SIZE]
            values = kv_ref[band, kv_width + group * HEAD_SIZE : kv_width + (group + 1) * HEAD_SIZE]
            first = group * group_size
            queries = jnp.concatenate(
                [
                    query_ref[rows, head * HEAD_SIZE : (head + 1) * HEAD_SIZE]
                    for head in range(first, first + group_size)
                ],
                axis=0,
            )
            scores = lax.dot_general(
                keys, queries, (((1,), (1,)), ((), ())), preferred_element_type=jnp.float32
            )
            scores = scores * (HEAD_SIZE ** (-0.5) * LOG2E) + bias_ref[group] + mask
            largest = jnp.max(scores, axis=0, keepdims=True)
            weight = jnp.exp2(scores - largest)
            total = jnp.sum(weight, axis=0, keepdims=True)
            blended = lax.dot_general(
                values,
                weight.astype(jnp.bfloat16),
                (((0,), (0,)), ((), ())),
                preferred_element_type=jnp.float32,
            )
            blended = blended / total
            for pair in range(group_size // 2):
                turned = jnp.transpose(blended[:, pair * LANES : (pair + 1) * LANES])
                both = jnp.concatenate([turned[:SEG], turned[SEG:]], axis=1)
                column = (first + 2 * pair) * HEAD_SIZE
                mixed_ref[rows, column : column + LANES] = both.astype(jnp.bfloat16)


def kernel(
    n_sp,
    residual_ref,
    query_ref,
    key_ref,
    value_ref,
    docs_ref,
    bias_one_ref,
    bias_two_ref,
    gain_ref,
    out_one_hbm,
    query_w_hbm,
    key_w_hbm,
    value_w_hbm,
    out_two_hbm,
    result_ref,
    w_out_one,
    w_query,
    w_kv,
    w_out_two,
    kv_one,
    kv_two,
    docs_prior,
    docs_col,
    mask,
    table_one,
    table_two,
    mixed,
    query_two,
    residual_full,
    part_own,
    part_in,
    layer,
    send_sem,
    recv_sem,
    load_sem,
):
    me = lax.axis_index("sp")
    my_tp = lax.axis_index("tp")
    other = 1 - my_tp
    tok_rows = residual_ref.shape[0]
    kv_width = key_ref.shape[1]
    chunks, _, wide = part_own.shape
    half = chunks // 2
    hops = hops_of(tok_rows)

    barrier = pltpu.get_barrier_semaphore()
    expected = jnp.int32(1)
    for distance, _, _, _ in hops:
        for step, there in ((distance, me + distance < n_sp), (-distance, me >= distance)):
            expected = expected + there.astype(jnp.int32)

            @pl.when(there)
            def _():
                pl.semaphore_signal(
                    barrier, inc=1, device_id={"sp": me + step}, device_id_type=MESH
                )

    pl.semaphore_signal(barrier, inc=1, device_id={"tp": other}, device_id_type=MESH)

    loads = [
        pltpu.make_async_copy(out_one_hbm, w_out_one, load_sem.at[0]),
        pltpu.make_async_copy(key_w_hbm, w_kv.at[:, pl.ds(0, kv_width)], load_sem.at[1]),
        pltpu.make_async_copy(value_w_hbm, w_kv.at[:, pl.ds(kv_width, kv_width)], load_sem.at[2]),
        pltpu.make_async_copy(query_w_hbm, w_query, load_sem.at[3]),
        pltpu.make_async_copy(out_two_hbm, w_out_two, load_sem.at[4]),
    ]
    for load in loads:
        load.start()

    slot = iter(range(send_sem.shape[0]))

    def remote(src, dst, index, target):
        return pltpu.make_async_remote_copy(
            src_ref=src,
            dst_ref=dst,
            send_sem=send_sem.at[index],
            recv_sem=recv_sem.at[index],
            device_id=target,
            device_id_type=MESH,
        )

    pl.semaphore_wait(barrier, expected)

    first_copies = []
    for distance, row, needed, landing in hops:
        target = {"sp": lax.rem(me + distance, n_sp)}
        here, there = pl.ds(row, needed), pl.ds(landing, needed)
        copies = [
            remote(key_ref.at[here], kv_one.at[there, pl.ds(0, kv_width)], next(slot), target),
            remote(value_ref.at[here], kv_one.at[there, pl.ds(kv_width, kv_width)], next(slot), target),
            remote(docs_ref, docs_prior.at[distance - 1], next(slot), target),
        ]
        first_copies.append((distance, copies))

        @pl.when(me + distance < n_sp)
        def _():
            for copy in copies:
                copy.start()

        @pl.when(me < distance)
        def _():
            empty = jnp.zeros((needed, 2 * kv_width), jnp.bfloat16)
            kv_one[landing : landing + needed] = empty
            kv_two[landing : landing + needed] = empty
            docs_prior[distance - 1] = jnp.full((1, tok_rows), -1, jnp.int32)

    residual_copy = remote(residual_ref, residual_full.at[my_tp], next(slot), {"tp": other})
    residual_copy.start()
    residual_full[my_tp] = residual_ref[...]
    kv_one[SPAN:, :kv_width] = key_ref[...]
    kv_one[SPAN:, kv_width:] = value_ref[...]

    build_bias(bias_one_ref, table_one)
    build_bias(bias_two_ref, table_two)

    def start_sent(distance, copies):
        @pl.when(me + distance < n_sp)
        def _():
            for copy in copies:
                copy.start()

    def wait_arrived(distance, copies):
        @pl.when(me >= distance)
        def _():
            for copy in copies:
                copy.wait_recv()

    def wait_sent(distance, copies):
        @pl.when(me + distance < n_sp)
        def _():
            for copy in copies:
                copy.wait_send()

    for distance, copies in first_copies:
        wait_arrived(distance, copies)

    eye = lax.broadcasted_iota(jnp.int32, (SEG, SEG), 0) == lax.broadcasted_iota(
        jnp.int32, (SEG, SEG), 1
    )

    def put_column(docs, place):
        picked = jnp.where(eye, docs.astype(jnp.float32), 0.0)
        docs_col[place : place + SEG] = jnp.broadcast_to(
            jnp.sum(picked, axis=1, keepdims=True), (SEG, LANES)
        )

    for distance, row, needed, landing in hops:
        for block in range(0, needed, SEG):
            put_column(
                docs_prior[distance - 1, :, row + block : row + block + SEG], landing + block
            )
    for block in range(0, tok_rows, SEG):
        put_column(docs_ref[:, block : block + SEG], SPAN + block)
    for segment in range(tok_rows // SEG):
        own = docs_ref[:, segment * SEG : (segment + 1) * SEG].astype(jnp.float32)
        own = jnp.concatenate([own, own], axis=1)
        same = docs_col[segment * SEG : segment * SEG + BAND] == own
        mask[segment] = jnp.where(same, 0.0, HIDDEN)

    attend(query_ref, kv_one, table_one, mask, mixed)

    loads[0].wait()
    part_copies = []
    for chunk in range(chunks):
        part_own[chunk] = jnp.dot(
            mixed[...],
            w_out_one[:, chunk * wide : (chunk + 1) * wide],
            preferred_element_type=jnp.float32,
        ).astype(jnp.bfloat16)
        copy = remote(part_own.at[chunk], part_in.at[chunk], next(slot), {"tp": other})
        copy.start()
        part_copies.append(copy)

    residual_copy.wait_recv()
    squares = jnp.zeros((tok_rows, 1), jnp.float32)
    for chunk in range(chunks):
        part_copies[chunk].wait_recv()
        column = (chunk % half) * wide
        rows = residual_full[chunk // half, :, column : column + wide].astype(jnp.float32)
        rows = rows + (
            part_own[chunk].astype(jnp.float32) + part_in[chunk].astype(jnp.float32)
        )
        rows = rows.astype(jnp.bfloat16)
        layer[chunk] = rows
        rows = rows.astype(jnp.float32)
        squares = squares + jnp.sum(rows * rows, axis=1, keepdims=True)
    scale = lax.rsqrt(squares / (chunks * wide) + eps)
    normed = jnp.concatenate(
        [
            (
                layer[chunk].astype(jnp.float32)
                * scale
                * gain_ref[:, chunk * wide : (chunk + 1) * wide]
            ).astype(jnp.bfloat16)
            for chunk in range(chunks)
        ],
        axis=1,
    )
    loads[1].wait()
    loads[2].wait()
    kv_two[SPAN:] = jnp.dot(normed, w_kv[...], preferred_element_type=jnp.float32).astype(
        jnp.bfloat16
    )
    second_copies = []
    for distance, row, needed, landing in hops:
        target = {"sp": lax.rem(me + distance, n_sp)}
        copies = [
            remote(
                kv_two.at[pl.ds(SPAN + row, needed)],
                kv_two.at[pl.ds(landing, needed)],
                next(slot),
                target,
            )
        ]
        second_copies.append((distance, copies))
        start_sent(distance, copies)
    loads[3].wait()
    query_two[...] = jnp.dot(normed, w_query[...], preferred_element_type=jnp.float32).astype(
        jnp.bfloat16
    )
    for copy in part_copies:
        copy.wait_send()
    for distance, copies in second_copies:
        wait_arrived(distance, copies)

    attend(query_two, kv_two, table_two, mask, mixed)

    loads[4].wait()
    last_copies = []
    for chunk in range(half):
        column = pl.multiple_of((other * half + chunk) * wide, wide)
        part_own[chunk] = jnp.dot(
            mixed[...], w_out_two[:, pl.ds(column, wide)], preferred_element_type=jnp.float32
        ).astype(jnp.bfloat16)
        copy = remote(part_own.at[chunk], part_in.at[chunks + chunk], next(slot), {"tp": other})
        copy.start()
        last_copies.append(copy)
    for chunk in range(half):
        column = pl.multiple_of((my_tp * half + chunk) * wide, wide)
        part_own[half + chunk] = jnp.dot(
            mixed[...], w_out_two[:, pl.ds(column, wide)], preferred_element_type=jnp.float32
        ).astype(jnp.bfloat16)
    for chunk in range(half):
        last_copies[chunk].wait_recv()
        branch = part_own[half + chunk].astype(jnp.float32) + part_in[chunks + chunk].astype(
            jnp.float32
        )
        result_ref[:, chunk * wide : (chunk + 1) * wide] = (
            layer[my_tp * half + chunk].astype(jnp.float32) + branch
        ).astype(jnp.bfloat16)

    residual_copy.wait_send()
    for distance, copies in first_copies + second_copies:
        wait_sent(distance, copies)
    for copy in last_copies:
        copy.wait_send()


def body(
    residual,
    query_first,
    key_first,
    value_first,
    documents,
    bias_first,
    out_first,
    norm_gain,
    query_w,
    key_w,
    value_w,
    bias_second,
    out_second,
):
    n_sp = lax.axis_size("sp")
    tok_rows, width_local = residual.shape
    query_width = query_first.shape[1]
    kv_width = key_first.shape[1]
    kv_local = kv_width // HEAD_SIZE
    group_width = query_width // kv_local
    wide = width_local // 2
    chunks = out_first.shape[1] // wide
    hops = len(hops_of(tok_rows))
    n_sems = 3 * hops + 1 + chunks + hops + chunks // 2
    vmem = pl.BlockSpec(memory_space=pltpu.VMEM)
    hbm = pl.BlockSpec(memory_space=pl.ANY)
    bf16 = jnp.bfloat16
    return pl.pallas_call(
        functools.partial(kernel, n_sp),
        name="two_layers",
        out_shape=jax.ShapeDtypeStruct((tok_rows, width_local), bf16),
        in_specs=[vmem] * 8 + [hbm] * 5,
        out_specs=vmem,
        scratch_shapes=[
            pltpu.VMEM(out_first.shape, bf16),
            pltpu.VMEM(query_w.shape, bf16),
            pltpu.VMEM((key_w.shape[0], 2 * kv_width), bf16),
            pltpu.VMEM(out_second.shape, bf16),
            pltpu.VMEM((SPAN + tok_rows, 2 * kv_width), bf16),
            pltpu.VMEM((SPAN + tok_rows, 2 * kv_width), bf16),
            pltpu.VMEM((hops, 1, tok_rows), jnp.int32),
            pltpu.VMEM((SPAN + tok_rows, LANES), jnp.float32),
            pltpu.VMEM((tok_rows // SEG, BAND, LANES), jnp.float32),
            pltpu.VMEM((kv_local, BAND, group_width), jnp.float32),
            pltpu.VMEM((kv_local, BAND, group_width), jnp.float32),
            pltpu.VMEM((tok_rows, query_width), bf16),
            pltpu.VMEM((tok_rows, query_width), bf16),
            pltpu.VMEM((2, tok_rows, width_local), bf16),
            pltpu.VMEM((chunks, tok_rows, wide), bf16),
            pltpu.VMEM((chunks + chunks // 2, tok_rows, wide), bf16),
            pltpu.VMEM((chunks, tok_rows, wide), bf16),
            pltpu.SemaphoreType.DMA((n_sems,)),
            pltpu.SemaphoreType.DMA((n_sems,)),
            pltpu.SemaphoreType.DMA((5,)),
        ],
        compiler_params=pltpu.CompilerParams(collective_id=0, has_side_effects=True),
    )(
        residual,
        query_first,
        key_first,
        value_first,
        documents.reshape(1, tok_rows),
        bias_first,
        bias_second,
        norm_gain.reshape(1, -1),
        out_first,
        query_w,
        key_w,
        value_w,
        out_second,
    )


def solution(mesh):
    placed = (
        P("sp", "tp"),
        P("sp", "tp"),
        P("sp", "tp"),
        P("sp", "tp"),
        P("sp"),
        P("tp", None),
        P("tp", None),
        P(),
        P(None, "tp"),
        P(None, "tp"),
        P(None, "tp"),
        P("tp", None),
        P("tp", None),
    )
    return jax.shard_map(body, mesh=mesh, in_specs=placed, out_specs=P("sp", "tp"), check_vma=False)
```

time: 160 us -> 23.6 us (0.15)
  local copies, waits for them, and re-layouts: 73.5 us -> 1.62 us
  starting transfers between devices: 22.4 us -> 0 us
  Pallas kernels: 0 us -> 21.6 us
  waiting for transfers between devices: 17.1 us -> 0 us
  matrix products: 16.2 us -> 0 us
  between operations: 14.7 us -> 0.01 us
  other arithmetic: 10.2 us -> 0 us
  blocking collectives: 4.37 us -> 0 us
    unnamed x316 -> x1, local copies, waits for them, and re-layouts: 40.1 us -> 1.62 us
    ppermute x10 -> x0, starting transfers between devices: 22.1 us -> none  [from_behind(): return lax.ppermute(block, axis, route)]
    pallas_call x0 -> x1, Pallas kernels: none -> 21.6 us  [body(): pl.pallas_call(functools.partial(kernel, n_sp), name='two_layers', out_sh...]
    another operation x130 -> x0, local copies, waits for them, and re-layouts: 15.2 us -> none  [bias_block(): return jnp.stack(rows, axis=1)]
    reduce_scatter x2 -> x0, waiting for transfers between devices: 12.9 us -> none  [the longest x1 12.9 us: body(): lax.psum_scatter(partial_two.astype(jnp.bfloat16), 'tp', scatter_dimensio...]
    dot_general x7 -> x0, matrix products: 9.58 us -> none  [the longest x2 5.32 us: attend(): jnp.einsum('skgqb,sbkd->sqkgd', softmax_weight, value_bands, preferred_el...]
    concatenate x49 -> x0, local copies, waits for them, and re-layouts: 9.34 us -> none  [the longest x46 8.58 us: make_bands(): jnp.concatenate([blocks[lag:lag + segments] for lag in range(PAST + 1)],...]
    slice x15 -> x0, local copies, waits for them, and re-layouts: 7.21 us -> none  [the longest x2 1.6 us: bias_block(): bias_table[:, table_cols - 1:]]
  transfers between devices with their start and end apart: 12 -> 0, of which waited for: 3 -> 0; matrix products, arithmetic and copies ran while one was open for 48% -> 0% of each run, Pallas kernels for 0% -> 0%
where the time goes in v1:
time: 23.6 us; the launch traced here: 23.2 us
  Pallas kernels  21.6 us (92%)
  local copies, waits for them, and re-layouts  1.62 us (7%)
    pallas_call x1, Pallas kernels, body(): pl.pallas_call(functools.partial(kernel, n_sp), name='two_layers', out_sh...  21.6 us
    unnamed x1, local copies, waits for them, and re-layouts  1.62 us

profile of v1, /device:TPU:25, one launch (start us, length us, event | category | flops | bytes accessed | tf_op | source)
XLA Modules:
  0.0 23.2 jit_solution(1001865468510088723)
XLA Ops:
  0.0 21.6 %two_layers.1 = bf16[192,512]{1,0:T(8,128)(2,1)} custom-call(bf16[192,512]{1,0:T(8,128)(2,1)} %residual_ref.1, bf16[192,512]{1,0:T(8,128)(2,1)} %query_ref.1, bf16[192,128]{1,0:T(8,128)(2,1)} %key_ref.1, bf16[192,128]{1,0:T(8,128)(2,1)} %value_ref.1, s32[1,192]{1,0:T(1,128)} %bitcast.3, f32[8,513]{1,0:T(8,128)} %bias_one_ref.1, f32[8,513]{1,0:T(8,128)} %bias_two_ref.1, ...), custom_call_target="tpu_custom_call" | custom-call | tf_op jit(solution)/shard_map/two_layers/pallas_call | solution.py:392
  21.6 1.6 %copy.15 = bf16[192,512]{1,0:T(8,128)(2,1)} copy(bf16[192,512]{1,0:T(8,128)(2,1)} %two_layers.1) | data formatting | bytes 393216

commit v2 on v1

v2 whole, which is shorter than its diff:
```python
import functools

import jax
import jax.numpy as jnp
from jax import lax
from jax.experimental import pallas as pl
from jax.experimental.pallas import tpu as pltpu
from jax.sharding import PartitionSpec as P

HEAD_SIZE = 64
SEG = 64
PAST = 4
REL_CLIP = 256
SPAN = PAST * SEG
BAND = SPAN + SEG
LANES = 128
LOG2E = 1.4426950408889634
HIDDEN = -1e30
MESH = pl.DeviceIdType.MESH


eps = 1e-06


def hops_of(tok_rows):
    return range(1, (SPAN + tok_rows - 1) // tok_rows + 1)


def pieces_of(tok_rows):
    pieces = []
    for distance in hops_of(tok_rows):
        top = SPAN - (distance - 1) * tok_rows
        bottom = max(0, top - tok_rows)
        cuts = [cut for cut in range(SEG, tok_rows, SEG) if bottom < cut < top]
        edges = [bottom] + cuts + [top]
        for low, high in reversed(list(zip(edges[:-1], edges[1:]))):
            pieces.append((distance, tok_rows - (top - low), high - low, low))
    return pieces


def build_bias(table_ref, bias_ref):
    heads_local = table_ref.shape[0]
    group_size = bias_ref.shape[2] // SEG
    lane = lax.broadcasted_iota(jnp.int32, (SEG, LANES), 1)
    low = lane < SEG
    last = REL_CLIP + SPAN

    def tile(head, index):
        if index == 0:
            return jnp.broadcast_to(table_ref[head : head + 1, last : last + 1], (SEG, LANES))
        first = last - index * LANES
        return jnp.broadcast_to(table_ref[head : head + 1, first : first + LANES], (SEG, LANES))

    def piece(head, block, base):
        back = block // 2
        if block % 2 == 0:
            source = jnp.where(low, tile(head, back), tile(head, back + 1))
            shift = base
        else:
            source = tile(head, back + 1)
            shift = (base + SEG) % LANES
        return pltpu.roll(source, shift, 1, stride=1, stride_axis=0)

    for head in range(0, heads_local, 2):
        for block in range(PAST + 1):
            pair = jnp.where(low, piece(head, block, 0), piece(head + 1, block, SEG)) * LOG2E
            group, inner = head // group_size, head % group_size
            bias_ref[group, block * SEG : (block + 1) * SEG, inner * SEG : (inner + 2) * SEG] = pair


def attend(segments, query_ref, kv_ref, bias_ref, mask_ref, mixed_ref):
    kv_local = bias_ref.shape[0]
    group_size = bias_ref.shape[2] // SEG
    kv_width = kv_local * HEAD_SIZE
    for segment in segments:
        rows = slice(segment * SEG, (segment + 1) * SEG)
        band = slice(segment * SEG, segment * SEG + BAND)
        mask = mask_ref[segment]
        mask = jnp.concatenate([mask] * (group_size * SEG // LANES), axis=1)
        for group in range(kv_local):
            keys = kv_ref[band, group * HEAD_SIZE : (group + 1) * HEAD_SIZE]
            values = kv_ref[band, kv_width + group * HEAD_SIZE : kv_width + (group + 1) * HEAD_SIZE]
            first = group * group_size
            queries = jnp.concatenate(
                [
                    query_ref[rows, head * HEAD_SIZE : (head + 1) * HEAD_SIZE]
                    for head in range(first, first + group_size)
                ],
                axis=0,
            )
            scores = lax.dot_general(
                keys, queries, (((1,), (1,)), ((), ())), preferred_element_type=jnp.float32
            )
            scores = scores * (HEAD_SIZE ** (-0.5) * LOG2E) + bias_ref[group] + mask
            largest = jnp.max(scores, axis=0, keepdims=True)
            weight = jnp.exp2(scores - largest)
            total = jnp.sum(weight, axis=0, keepdims=True)
            blended = lax.dot_general(
                values,
                weight.astype(jnp.bfloat16),
                (((0,), (0,)), ((), ())),
                preferred_element_type=jnp.float32,
            )
            blended = blended / total
            for pair in range(group_size // 2):
                turned = jnp.transpose(blended[:, pair * LANES : (pair + 1) * LANES])
                both = jnp.concatenate([turned[:SEG], turned[SEG:]], axis=1)
                column = (first + 2 * pair) * HEAD_SIZE
                mixed_ref[rows, column : column + LANES] = both.astype(jnp.bfloat16)


def kernel(
    n_sp,
    key_ref,
    value_ref,
    docs_ref,
    bias_one_ref,
    bias_two_ref,
    gain_ref,
    residual_hbm,
    query_hbm,
    out_one_hbm,
    query_w_hbm,
    key_w_hbm,
    value_w_hbm,
    out_two_hbm,
    result_ref,
    w_out_one,
    w_query,
    w_kv,
    w_out_two,
    kv_one,
    kv_two,
    docs_prior,
    docs_col,
    mask,
    table_one,
    table_two,
    mixed,
    query_one,
    query_two,
    residual_full,
    part_own,
    part_in,
    last_in,
    layer,
    normed,
    send_sem,
    recv_sem,
    load_sem,
):
    me = lax.axis_index("sp")
    my_tp = lax.axis_index("tp")
    other = 1 - my_tp
    tok_rows, width_local = residual_hbm.shape
    kv_width = key_ref.shape[1]
    segments = tok_rows // SEG
    hops = hops_of(tok_rows)
    pieces = pieces_of(tok_rows)
    halves = part_own.shape[0]
    blocks = [(range(segments - 1, 0, -1), SEG, tok_rows - SEG), (range(1), 0, SEG)]

    barrier = pltpu.get_barrier_semaphore()
    expected = jnp.int32(1)
    for distance in hops:
        for step, there in ((distance, me + distance < n_sp), (-distance, me >= distance)):
            expected = expected + there.astype(jnp.int32)

            @pl.when(there)
            def _():
                pl.semaphore_signal(
                    barrier, inc=1, device_id={"sp": me + step}, device_id_type=MESH
                )

    pl.semaphore_signal(barrier, inc=1, device_id={"tp": other}, device_id_type=MESH)

    loads = [
        pltpu.make_async_copy(query_hbm, query_one, load_sem.at[0]),
        pltpu.make_async_copy(out_one_hbm, w_out_one, load_sem.at[1]),
        pltpu.make_async_copy(residual_hbm, residual_full.at[my_tp], load_sem.at[2]),
        pltpu.make_async_copy(key_w_hbm, w_kv.at[:, pl.ds(0, kv_width)], load_sem.at[3]),
        pltpu.make_async_copy(value_w_hbm, w_kv.at[:, pl.ds(kv_width, kv_width)], load_sem.at[4]),
        pltpu.make_async_copy(query_w_hbm, w_query, load_sem.at[5]),
        pltpu.make_async_copy(out_two_hbm, w_out_two, load_sem.at[6]),
    ]
    for load in loads:
        load.start()

    slot = iter(range(send_sem.shape[0]))

    def remote(src, dst, target):
        index = next(slot)
        return pltpu.make_async_remote_copy(
            src_ref=src,
            dst_ref=dst,
            send_sem=send_sem.at[index],
            recv_sem=recv_sem.at[index],
            device_id=target,
            device_id_type=MESH,
        )

    def ahead(distance):
        return {"sp": lax.rem(me + distance, n_sp)}

    def start_sent(distance, copies):
        @pl.when(me + distance < n_sp)
        def _():
            for copy in copies:
                copy.start()

    def wait_arrived(distance, copies):
        @pl.when(me >= distance)
        def _():
            for copy in copies:
                copy.wait_recv()

    def wait_sent(distance, copies):
        @pl.when(me + distance < n_sp)
        def _():
            for copy in copies:
                copy.wait_send()

    pl.semaphore_wait(barrier, expected)

    docs_copies = []
    for distance in hops:
        copies = [remote(docs_ref, docs_prior.at[distance - 1], ahead(distance))]
        docs_copies.append((distance, copies))
        start_sent(distance, copies)
    first_copies = []
    for distance, row, needed, landing in pieces:
        here, there = pl.ds(row, needed), pl.ds(landing, needed)
        copies = [
            remote(key_ref.at[here], kv_one.at[there, pl.ds(0, kv_width)], ahead(distance)),
            remote(value_ref.at[here], kv_one.at[there, pl.ds(kv_width, kv_width)], ahead(distance)),
        ]
        first_copies.append((distance, copies))
        start_sent(distance, copies)
    residual_copy = remote(residual_hbm, residual_full.at[my_tp], {"tp": other})
    residual_copy.start()

    for distance, _, needed, landing in pieces:

        @pl.when(me < distance)
        def _():
            empty = jnp.zeros((needed, 2 * kv_width), jnp.bfloat16)
            kv_one[landing : landing + needed] = empty
            kv_two[landing : landing + needed] = empty

    for distance in hops:

        @pl.when(me < distance)
        def _():
            docs_prior[distance - 1] = jnp.full((1, tok_rows), -1, jnp.int32)

    kv_one[SPAN:, :kv_width] = key_ref[...]
    kv_one[SPAN:, kv_width:] = value_ref[...]

    build_bias(bias_one_ref, table_one)
    build_bias(bias_two_ref, table_two)

    for distance, copies in docs_copies:
        wait_arrived(distance, copies)

    eye = lax.broadcasted_iota(jnp.int32, (SEG, SEG), 0) == lax.broadcasted_iota(
        jnp.int32, (SEG, SEG), 1
    )

    def put_column(docs, place):
        picked = jnp.where(eye, docs.astype(jnp.float32), 0.0)
        docs_col[place : place + SEG] = jnp.broadcast_to(
            jnp.sum(picked, axis=1, keepdims=True), (SEG, LANES)
        )

    for distance, row, needed, landing in pieces:
        for block in range(0, needed, SEG):
            put_column(
                docs_prior[distance - 1, :, row + block : row + block + SEG], landing + block
            )
    for block in range(0, tok_rows, SEG):
        put_column(docs_ref[:, block : block + SEG], SPAN + block)
    for segment in range(segments):
        own = docs_ref[:, segment * SEG : (segment + 1) * SEG].astype(jnp.float32)
        own = jnp.concatenate([own, own], axis=1)
        same = docs_col[segment * SEG : segment * SEG + BAND] == own
        mask[segment] = jnp.where(same, 0.0, HIDDEN)

    def attend_block(members, waiting, *refs):
        for segment in members:
            for (distance, _, needed, landing), (_, copies) in zip(pieces, waiting):
                reached = landing + needed > segment * SEG
                earlier = landing + needed > (segment + 1) * SEG
                if reached and not (earlier and segment + 1 < segments):
                    wait_arrived(distance, copies)
            attend([segment], *refs)

    loads[0].wait()
    part_copies = []
    for members, start, count in blocks:
        attend_block(members, first_copies, query_one, kv_one, table_one, mask, mixed)
        if start > 0:
            loads[1].wait()
        rows = pl.ds(start, count)
        copies = []
        for half in range(halves):
            part_own[half, start : start + count] = jnp.dot(
                mixed[start : start + count],
                w_out_one[:, half * width_local : (half + 1) * width_local],
                preferred_element_type=jnp.float32,
            ).astype(jnp.bfloat16)
            copy = remote(part_own.at[half, rows], part_in.at[half, rows], {"tp": other})
            copy.start()
            copies.append(copy)
        part_copies.append(copies)

    loads[2].wait()
    residual_copy.wait_recv()
    second_copies = [None] * len(pieces)
    for (_, start, count), copies in zip(blocks, part_copies):
        rows = slice(start, start + count)
        squares = jnp.zeros((count, 1), jnp.float32)
        for half in range(halves):
            copies[half].wait_recv()
            new = residual_full[half, rows].astype(jnp.float32) + (
                part_own[half, rows].astype(jnp.float32) + part_in[half, rows].astype(jnp.float32)
            )
            new = new.astype(jnp.bfloat16)
            layer[half, rows] = new
            new = new.astype(jnp.float32)
            squares = squares + jnp.sum(new * new, axis=1, keepdims=True)
        scale = lax.rsqrt(squares / (halves * width_local) + eps)
        for half in range(halves):
            columns = slice(half * width_local, (half + 1) * width_local)
            normed[rows, columns] = (
                layer[half, rows].astype(jnp.float32) * scale * gain_ref[:, columns]
            ).astype(jnp.bfloat16)
        if start > 0:
            loads[3].wait()
            loads[4].wait()
        kv_two[SPAN + start : SPAN + start + count] = jnp.dot(
            normed[rows], w_kv[...], preferred_element_type=jnp.float32
        ).astype(jnp.bfloat16)
        for index, (distance, row, needed, landing) in enumerate(pieces):
            if start <= row < start + count:
                piece = remote(
                    kv_two.at[pl.ds(SPAN + row, needed)],
                    kv_two.at[pl.ds(landing, needed)],
                    ahead(distance),
                )
                second_copies[index] = (distance, [piece])
                start_sent(distance, [piece])
    loads[5].wait()
    query_two[...] = jnp.dot(normed[...], w_query[...], preferred_element_type=jnp.float32).astype(
        jnp.bfloat16
    )
    for copies in part_copies:
        for copy in copies:
            copy.wait_send()

    loads[6].wait()
    theirs = pl.ds(pl.multiple_of(other * width_local, width_local), width_local)
    ours = pl.ds(pl.multiple_of(my_tp * width_local, width_local), width_local)
    last_copies = []
    for members, start, count in blocks:
        attend_block(members, second_copies, query_two, kv_two, table_two, mask, mixed)
        rows = pl.ds(start, count)
        part_own[0, start : start + count] = jnp.dot(
            mixed[start : start + count], w_out_two[:, theirs], preferred_element_type=jnp.float32
        ).astype(jnp.bfloat16)
        copy = remote(part_own.at[0, rows], last_in.at[rows], {"tp": other})
        copy.start()
        last_copies.append(copy)
    part_own[1] = jnp.dot(
        mixed[...], w_out_two[:, ours], preferred_element_type=jnp.float32
    ).astype(jnp.bfloat16)
    for (_, start, count), copy in zip(blocks, last_copies):
        rows = slice(start, start + count)
        copy.wait_recv()
        branch = part_own[1, rows].astype(jnp.float32) + last_in[rows].astype(jnp.float32)
        result_ref[rows] = (layer[my_tp, rows].astype(jnp.float32) + branch).astype(jnp.bfloat16)

    residual_copy.wait_send()
    for distance, copies in docs_copies + first_copies + second_copies:
        wait_sent(distance, copies)
    for copy in last_copies:
        copy.wait_send()


def body(
    residual,
    query_first,
    key_first,
    value_first,
    documents,
    bias_first,
    out_first,
    norm_gain,
    query_w,
    key_w,
    value_w,
    bias_second,
    out_second,
):
    n_sp = lax.axis_size("sp")
    tok_rows, width_local = residual.shape
    query_width = query_first.shape[1]
    kv_width = key_first.shape[1]
    kv_local = kv_width // HEAD_SIZE
    group_width = query_width // kv_local
    halves = out_first.shape[1] // width_local
    hops = len(hops_of(tok_rows))
    n_sems = hops + 3 * len(pieces_of(tok_rows)) + 1 + 2 * halves + 2
    vmem = pl.BlockSpec(memory_space=pltpu.VMEM)
    hbm = pl.BlockSpec(memory_space=pl.ANY)
    bf16 = jnp.bfloat16
    return pl.pallas_call(
        functools.partial(kernel, n_sp),
        name="two_layers",
        out_shape=pltpu.VMEM((tok_rows, width_local), bf16),
        in_specs=[vmem] * 6 + [hbm] * 7,
        out_specs=vmem,
        scratch_shapes=[
            pltpu.VMEM(out_first.shape, bf16),
            pltpu.VMEM(query_w.shape, bf16),
            pltpu.VMEM((key_w.shape[0], 2 * kv_width), bf16),
            pltpu.VMEM(out_second.shape, bf16),
            pltpu.VMEM((SPAN + tok_rows, 2 * kv_width), bf16),
            pltpu.VMEM((SPAN + tok_rows, 2 * kv_width), bf16),
            pltpu.VMEM((hops, 1, tok_rows), jnp.int32),
            pltpu.VMEM((SPAN + tok_rows, LANES), jnp.float32),
            pltpu.VMEM((tok_rows // SEG, BAND, LANES), jnp.float32),
            pltpu.VMEM((kv_local, BAND, group_width), jnp.float32),
            pltpu.VMEM((kv_local, BAND, group_width), jnp.float32),
            pltpu.VMEM((tok_rows, query_width), bf16),
            pltpu.VMEM((tok_rows, query_width), bf16),
            pltpu.VMEM((tok_rows, query_width), bf16),
            pltpu.VMEM((halves, tok_rows, width_local), bf16),
            pltpu.VMEM((halves, tok_rows, width_local), bf16),
            pltpu.VMEM((halves, tok_rows, width_local), bf16),
            pltpu.VMEM((tok_rows, width_local), bf16),
            pltpu.VMEM((halves, tok_rows, width_local), bf16),
            pltpu.VMEM((tok_rows, halves * width_local), bf16),
            pltpu.SemaphoreType.DMA((n_sems,)),
            pltpu.SemaphoreType.DMA((n_sems,)),
            pltpu.SemaphoreType.DMA((7,)),
        ],
        compiler_params=pltpu.CompilerParams(collective_id=0, has_side_effects=True),
    )(
        key_first,
        value_first,
        documents.reshape(1, tok_rows),
        bias_first,
        bias_second,
        norm_gain.reshape(1, -1),
        residual,
        query_first,
        out_first,
        query_w,
        key_w,
        value_w,
        out_second,
    )


def solution(mesh):
    placed = (
        P("sp", "tp"),
        P("sp", "tp"),
        P("sp", "tp"),
        P("sp", "tp"),
        P("sp"),
        P("tp", None),
        P("tp", None),
        P(),
        P(None, "tp"),
        P(None, "tp"),
        P(None, "tp"),
        P("tp", None),
        P("tp", None),
    )
    return jax.shard_map(body, mesh=mesh, in_specs=placed, out_specs=P("sp", "tp"), check_vma=False)
```

time: 23.6 us -> 21.1 us (0.89)
  Pallas kernels: 21.6 us -> 20.2 us
  local copies, waits for them, and re-layouts: 1.62 us -> 0.68 us
    pallas_call x1, Pallas kernels: 21.6 us -> 20.2 us  [body(): pl.pallas_call(functools.partial(kernel, n_sp), name='two_layers', out_sh...]
    unnamed x1, local copies, waits for them, and re-layouts: 1.62 us -> 0.68 us
where the time goes in v2:
time: 21.1 us; the launch traced here: 20.9 us
  Pallas kernels  20.2 us (96%)
  local copies, waits for them, and re-layouts  0.68 us (3%)
    pallas_call x1, Pallas kernels, body(): pl.pallas_call(functools.partial(kernel, n_sp), name='two_layers', out_sh...  20.2 us
    unnamed x1, local copies, waits for them, and re-layouts  0.68 us

profile of v2, /device:TPU:25, one launch (start us, length us, event | category | flops | bytes accessed | tf_op | source)
XLA Modules:
  0.0 20.9 jit_solution(14482670849832382924)
XLA Ops:
  0.0 20.2 %two_layers.1 = bf16[192,512]{1,0:T(8,128)(2,1)S(1)} custom-call(bf16[192,128]{1,0:T(8,128)(2,1)} %key_ref.1, bf16[192,128]{1,0:T(8,128)(2,1)} %value_ref.1, s32[1,192]{1,0:T(1,128)} %bitcast.3, f32[8,513]{1,0:T(8,128)} %bias_one_ref.1, f32[8,513]{1,0:T(8,128)} %bias_two_ref.1, f32[1,1024]{1,0:T(1,128)} %bitcast.2, bf16[192,512]{1,0:T(8,128)(2,1)} %residual_hbm.1, ...), custom_call_target="tpu_custom_call" | custom-call | tf_op jit(solution)/shard_map/two_layers/pallas_call | solution.py:416
  20.2 0.7 %copy.15 = bf16[192,512]{1,0:T(8,128)(2,1)} copy(bf16[192,512]{1,0:T(8,128)(2,1)S(1)} %two_layers.1) | data formatting | bytes 393216
